TPU v7x, 32 devices: a whole 2x2x4 slice. The times are simulated.
32 devices in a mesh: ep: 8 (over z, x), tp: 4 (over y, core).
Axes of the slice: x: 2, y: 2, z: 4, core: 2. Of those that a mesh axis runs over, the one named last changes fastest.
Arguments:
- tokens: bfloat16 [4096, 4096], P('ep', 'tp'), may hold values from -100 to 100, as said below
- routes: int32 [4096, 2], P('ep'), may hold values from 0 to 15, all different within a row; in each aligned block of 512 rows (0 to 511, 512 to 1023, ...) at most 128 rows name the same one
- route_weights: float32 [4096, 2], P('ep'), may hold values from 0.1 to 1
- norm_gain: float32 [4096], P('tp'), may hold values from 0.1 to 1.9
- gate_weight: bfloat16 [16, 4096, 512], P('ep', 'tp'), may hold values from -0.09375 to 0.09375
- up_weight: bfloat16 [16, 4096, 512], P('ep', 'tp'), may hold values from -0.09375 to 0.09375
- down_weight: bfloat16 [16, 512, 4096], P('ep', None, 'tp'), may hold values from -0.25 to 0.25
- final_gain: float32 [4096], P('tp'), may hold values from 0.1 to 1.9
Outputs:
- mixed: bfloat16 [4096, 4096], P('ep', 'tp')
Inputs may be any that keep to these rules, and one draw needn't show every extreme that they name: `tokens`: real-valued activations whose features differ in scale. `routes`: each row names 2 different experts; among the 512 rows of one aligned block no expert is named more than 128 times, a bound that some block reaches.
All inputs are finite; a program needn't handle non-finite values.
Results may differ from a plain program's by a relative error of at most 0.018.
Values may be sent and summed in bfloat16 or wider, within the bound.
A program may use at most 64 MiB of HBM per device.

v0:
```python
import jax
import jax.numpy as jnp
from jax import lax
from jax.sharding import PartitionSpec as P

D = 4096


EPSILON = 1e-06


def expert_rows(weights, block):
    w_gate, w_up, w_down = weights
    gate = jnp.einsum("scd,df->scf", block, w_gate, preferred_element_type=jnp.float32)
    upper = jnp.einsum("scd,df->scf", block, w_up, preferred_element_type=jnp.float32)
    gate_sum, upper_sum = (
        lax.psum_scatter(gate.astype(jnp.bfloat16), "tp", scatter_dimension=2, tiled=True).astype(
            jnp.float32
        ),
        lax.psum_scatter(upper.astype(jnp.bfloat16), "tp", scatter_dimension=2, tiled=True).astype(
            jnp.float32
        ),
    )
    share = (jax.nn.silu(gate_sum) * upper_sum).astype(jnp.bfloat16)
    hidden = lax.all_gather(share, "tp", axis=2, tiled=True)
    return jnp.einsum("scf,fd->scd", hidden, w_down, preferred_element_type=jnp.float32).astype(
        jnp.bfloat16
    )


def serve_single(weights, block):
    return lax.all_to_all(
        expert_rows(weights, block), "ep", split_axis=0, concat_axis=0, tiled=True
    )


def body(tokens, routes, route_weights, norm_gain, gate_weight, up_weight, down_weight, final_gain):
    ep_count = lax.axis_size("ep")
    local_count = gate_weight.shape[0]
    experts = ep_count * local_count
    tok_rows = tokens.shape[0]
    top_count = routes.shape[1]
    capacity = 4 * tok_rows // experts
    values = tokens.astype(jnp.float32)
    squares = lax.psum(jnp.sum(values * values, axis=-1), "tp")
    normed = (values * lax.rsqrt(squares / D + EPSILON)[:, None] * norm_gain).astype(jnp.bfloat16)
    chosen = routes.reshape(-1)
    onehot = (chosen[:, None] == jnp.arange(experts, dtype=jnp.int32)[None, :]).astype(jnp.int32)
    slots = jnp.sum((jnp.cumsum(onehot, axis=0) - onehot) * onehot, axis=1)
    target = chosen * capacity + slots
    owners = jnp.arange(tok_rows * top_count, dtype=jnp.int32) // top_count
    table = jnp.full((experts * capacity,), tok_rows, jnp.int32).at[target].set(owners)
    padded = jnp.concatenate([normed, jnp.zeros((1, normed.shape[1]), jnp.bfloat16)], axis=0)
    outgoing = padded[table].reshape(ep_count, local_count, capacity, normed.shape[1])
    weight_list = [
        (gate_weight[member], up_weight[member], down_weight[member])
        for member in range(local_count)
    ]
    pieces = []
    for member in range(local_count):
        pieces.append(
            serve_single(
                weight_list[member],
                lax.all_to_all(outgoing[:, member], "ep", split_axis=0, concat_axis=0, tiled=True),
            )
        )
    arrived = jnp.stack(pieces, axis=1)
    returned = arrived.reshape(experts * capacity, normed.shape[1])
    position = target.reshape(tok_rows, top_count)
    combined = jnp.zeros((tok_rows, normed.shape[1]), jnp.float32)
    for which in range(top_count):
        combined = combined + route_weights[:, which : which + 1] * returned[
            position[:, which]
        ].astype(jnp.float32)
    closing = lax.psum(jnp.sum(combined * combined, axis=-1), "tp")
    return (combined * lax.rsqrt(closing / D + EPSILON)[:, None] * final_gain).astype(jnp.bfloat16)


def solution(mesh):
    in_specs = (
        P("ep", "tp"),
        P("ep", None),
        P("ep", None),
        P("tp"),
        P("ep", "tp", None),
        P("ep", "tp", None),
        P("ep", None, "tp"),
        P("tp"),
    )
    out_specs = P("ep", "tp")
    return jax.shard_map(body, mesh=mesh, in_specs=in_specs, out_specs=out_specs, check_vma=False)
```

profile of v0, /device:TPU:0, one launch (start us, length us, event | category | flops | bytes accessed | tf_op | source)
XLA Modules:
  0.0 332.4 jit_solution(4399818030590045528)
XLA Ops:
  9.3 8.4 %psum.14 = f32[512]{0:T(512)S(1)} all-reduce(f32[512]{0:T(512)S(1)} %fusion), channel_id=1, replica_groups=mesh['ep'=8,'tp'=4] {'tp'}, use_global_device_ids=true, to_apply=%region_1.0 | all-reduce | flops 512 | bytes 4096 | tf_op jit(solution)/shard_map/psum | solution.py:45
  17.7 4.5 %reduce-window.6 = s32[16,8,128]{2,1,0:T(8,128)S(1)} reduce-window(s32[16,8,128]{2,1,0:T(8,128)S(1)} %fusion.30, s32[]{:T(128)} %constant.41.clone.1), window={size=1x1x128 pad=0_0x0_0x127_0}, to_apply=%region_2.0 | reduce-window | flops 2080768 | bytes 131076 | tf_op jit(solution)/shard_map/reduce-window
  23.1 4.3 %scatter_custom_fusion = s32[2048]{0:T(1024)S(1)} fusion(s32[1024]{0:T(1024)S(1)} %bitcast.128, s32[1024]{0:T(1024)S(1)} %add_select_fusion, s32[]{:T(128)} %constant.39.clone.1), kind=kCustom, calls=%fused_computation.75 | custom fusion | bytes 8196 | tf_op jit(solution)/shard_map/scatter | solution.py:52
  27.9 9.7 %gather_fusion = bf16[2048,1024]{1,0:T(8,128)(2,1)} fusion(bf16[513,1024]{1,0:T(8,128)(2,1)S(1)} %concatenate.3, s32[2048]{0:T(1024)S(1)} %fusion.31), kind=kCustom, calls=%fused_computation | custom fusion | bytes 8396800 | tf_op jit(solution)/shard_map/gather | solution.py:54
  37.6 4.0 %slice_bitcast_fusion.1 = (bf16[8,128,1024]{2,1,0:T(8,128)(2,1)}, bf16[8,128,1024]{2,1,0:T(8,128)(2,1)S(1)}) fusion(bf16[8,2,128,1024]{3,2,1,0:T(8,128)(2,1)} %bitcast.103), kind=kLoop, calls=%fused_computation.11 | loop fusion | bytes 8388608 | tf_op jit(solution)/shard_map/squeeze | solution.py:64
  41.7 52.7 %all_to_all.20 = bf16[8,128,1024]{2,1,0:T(8,128)(2,1)S(1)} all-to-all(bf16[8,128,1024]{2,1,0:T(8,128)(2,1)S(1)} %get-tuple-element.8), channel_id=1, replica_groups=mesh['ep'=8,'tp'=4] {'ep'}, dimensions={0} | all-to-all | bytes 4194304 | tf_op jit(solution)/shard_map/all_to_all | solution.py:64
  99.6 4.4 %all-to-all-start = ((bf16[8,128,1024]{2,1,0:T(8,128)(2,1)}), bf16[8,128,1024]{2,1,0:T(8,128)(2,1)}, u32[]{:S(2)}, u32[]{:S(2)}) async-start(bf16[8,128,1024]{2,1,0:T(8,128)(2,1)} %get-tuple-element.7), calls=%async_computation | async-start | bytes 4194304 | tf_op jit(solution)/shard_map/all_to_all | solution.py:64
  104.0 3.4 %convolution_convert_fusion.3 = bf16[8,128,512]{2,1,0:T(8,128)(2,1)} fusion(bf16[8,128,1024]{2,1,0:T(8,128)(2,1)S(1)} %all_to_all.20, bf16[2,1024,512]{2,1,0:T(8,128)(2,1)} %param.12), kind=kOutput, calls=%fused_computation.18 | convolution fusion | flops 1074266112 | bytes 4194304 | tf_op jit(solution)/shard_map/scd,df->scf/dot_general | solution.py:14
  110.5 13.1 %reduce-scatter.19.cloned.1.call-done = bf16[128,1024]{1,0:T(8,128)(2,1)} async-done(((bf16[512,1024]{1,0:T(8,128)(2,1)}), bf16[128,1024]{1,0:T(8,128)(2,1)}) %reduce-scatter.19.cloned.1.call-update) | async-done | bytes 262160
  124.9 26.1 %reduce-scatter.17.cloned.1.call-done = bf16[128,1024]{1,0:T(8,128)(2,1)} async-done(((bf16[512,1024]{1,0:T(8,128)(2,1)}), bf16[128,1024]{1,0:T(8,128)(2,1)}) %reduce-scatter.17.cloned.1.call-update) | async-done | bytes 262160
  153.2 3.1 convolution_convert_fusion.4
  158.4 3.2 convolution_convert_fusion.5
  163.7 6.5 %all-gather.5.cloned.1.call-done = bf16[8,128,512]{2,1,0:T(8,128)(2,1)} async-done(((bf16[8,128,128]{2,1,0:T(8,128)(2,1)}), bf16[8,128,512]{2,1,0:T(8,128)(2,1)}) %all-gather.5.cloned.1.call-update) | async-done | bytes 1048592 | tf_op jit(solution)/shard_map/all_gather | solution.py:25
  170.1 3.8 %convolution_convert_fusion = bf16[8,128,1024]{2,1,0:T(8,128)(2,1)} fusion(bf16[8,128,512]{2,1,0:T(8,128)(2,1)} %all-gather.5.cloned.1.call-done, bf16[2,512,1024]{2,1,0:T(8,128)(2,1)S(1)} %copy-done.5), kind=kOutput, calls=%fused_computation.15 | convolution fusion | flops 1074790400 | bytes 4194304 | tf_op jit(solution)/shard_map/scf,fd->scd/dot_general | solution.py:26
  174.0 5.5 %all-to-all-start.3 = ((bf16[8,128,1024]{2,1,0:T(8,128)(2,1)}), bf16[8,128,1024]{2,1,0:T(8,128)(2,1)S(1)}, u32[]{:S(2)}, u32[]{:S(2)}) async-start(bf16[8,128,1024]{2,1,0:T(8,128)(2,1)} %convolution_convert_fusion), calls=%async_computation.3 | async-start | bytes 4194304 | tf_op jit(solution)/shard_map/all_to_all | solution.py:32
  179.7 17.6 %reduce-scatter.15.cloned.1.call-done = bf16[128,1024]{1,0:T(8,128)(2,1)} async-done(((bf16[512,1024]{1,0:T(8,128)(2,1)}), bf16[128,1024]{1,0:T(8,128)(2,1)}) %reduce-scatter.15.cloned.1.call-update) | async-done | bytes 262160
  198.6 26.0 %reduce-scatter.13.cloned.1.call-done = bf16[128,1024]{1,0:T(8,128)(2,1)} async-done(((bf16[512,1024]{1,0:T(8,128)(2,1)}), bf16[128,1024]{1,0:T(8,128)(2,1)}) %reduce-scatter.13.cloned.1.call-update) | async-done | bytes 262160
  226.7 17.0 %all-gather.3.cloned.1.call-done = bf16[8,128,512]{2,1,0:T(8,128)(2,1)} async-done(((bf16[8,128,128]{2,1,0:T(8,128)(2,1)}), bf16[8,128,512]{2,1,0:T(8,128)(2,1)}) %all-gather.3.cloned.1.call-update) | async-done | bytes 1048592 | tf_op jit(solution)/shard_map/all_gather | solution.py:25
  243.6 4.1 %convolution_convert_fusion.1 = bf16[8,128,1024]{2,1,0:T(8,128)(2,1)} fusion(bf16[8,128,512]{2,1,0:T(8,128)(2,1)} %all-gather.3.cloned.1.call-done, bf16[2,512,1024]{2,1,0:T(8,128)(2,1)} %param.14), kind=kOutput, calls=%fused_computation.16 | convolution fusion | flops 1074790400 | bytes 4194304 | tf_op jit(solution)/shard_map/scf,fd->scd/dot_general | solution.py:26
  247.7 5.6 %all-to-all-start.1 = ((bf16[8,128,1024]{2,1,0:T(8,128)(2,1)}), bf16[8,128,1024]{2,1,0:T(8,128)(2,1)}, u32[]{:S(2)}, u32[]{:S(2)}) async-start(bf16[8,128,1024]{2,1,0:T(8,128)(2,1)} %convolution_convert_fusion.1), calls=%async_computation.1 | async-start | bytes 4194304 | tf_op jit(solution)/shard_map/all_to_all | solution.py:32
  253.7 48.4 %all-to-all-done.1 = bf16[8,128,1024]{2,1,0:T(8,128)(2,1)} async-done(((bf16[8,128,1024]{2,1,0:T(8,128)(2,1)}), bf16[8,128,1024]{2,1,0:T(8,128)(2,1)}, u32[]{:S(2)}, u32[]{:S(2)}) %all-to-all-start.1) | async-done | bytes 2097184 | tf_op jit(solution)/shard_map/all_to_all | solution.py:32
  306.5 5.5 %gather_fusion.2 = bf16[512,1024]{1,0:T(8,128)(2,1)S(1)} fusion(bf16[2048,1024]{1,0:T(8,128)(2,1)} %bitcast.101, s32[1024]{0:T(1024)S(1)} %get-tuple-element.13), kind=kCustom, calls=%fused_computation.2 | custom fusion | bytes 2099200 | tf_op jit(solution)/shard_map/gather | solution.py:72
  311.9 5.5 %gather_fusion.1 = bf16[512,1024]{1,0:T(8,128)(2,1)S(1)} fusion(bf16[2048,1024]{1,0:T(8,128)(2,1)} %bitcast.102, s32[1024]{0:T(1024)S(1)} %get-tuple-element.14), kind=kCustom, calls=%fused_computation.1 | custom fusion | bytes 2099200 | tf_op jit(solution)/shard_map/gather | solution.py:72
  318.0 5.9 %psum.15 = f32[512]{0:T(512)S(1)} all-reduce(f32[512]{0:T(512)S(1)} %multiply_reduce_fusion), channel_id=1, replica_groups=mesh['ep'=8,'tp'=4] {'tp'}, use_global_device_ids=true, to_apply=%region_11.12 | all-reduce | flops 512 | bytes 4096 | tf_op jit(solution)/shard_map/psum | solution.py:75
  (74 shorter events, 30.2 us)
Async XLA Ops:
  6.5 21.0 %copy-start = (bf16[512,1024]{1,0:T(8,128)(2,1)S(1)}, bf16[512,1024]{1,0:T(8,128)(2,1)}, u32[]{:S(2)}) copy-start(bf16[512,1024]{1,0:T(8,128)(2,1)} %param.8) | copy-start | bytes 3145732
  6.5 21.0 %copy-start.1 = (f32[1024]{0:T(1024)S(1)}, f32[1024]{0:T(1024)}, u32[]{:S(2)}) copy-start(f32[1024]{0:T(1024)} %param.11) | copy-start | bytes 12292
  6.5 117.1 %reduce-scatter.19.cloned.1.call-start = ((), (), s32[]{:S(2)}) async-start(), calls=%async_computation.13 | async-start | bytes 1310720
  41.6 52.7 %copy-start.4 = (bf16[2,1024,512]{2,1,0:T(8,128)(2,1)S(1)}, bf16[2,1024,512]{2,1,0:T(8,128)(2,1)}, u32[]{:S(2)}) copy-start(bf16[2,1024,512]{2,1,0:T(8,128)(2,1)} %param.13) | copy-start | bytes 6291460
  99.6 53.6 %all-to-all-start = ((bf16[8,128,1024]{2,1,0:T(8,128)(2,1)}), bf16[8,128,1024]{2,1,0:T(8,128)(2,1)}, u32[]{:S(2)}, u32[]{:S(2)}) async-start(bf16[8,128,1024]{2,1,0:T(8,128)(2,1)} %get-tuple-element.7), calls=%async_computation | async-start | bytes 4194304 | tf_op jit(solution)/shard_map/all_to_all | solution.py:64
  104.0 47.0 %reduce-scatter.17.cloned.1.call-start = ((), (), s32[]{:S(2)}) async-start(), calls=%async_computation.12 | async-start | bytes 1310720
  110.5 59.6 %all-gather.5.cloned.1.call-start = ((), (), s32[]{:S(2)}) async-start(), calls=%async_computation.9 | async-start | bytes 1310720 | tf_op jit(solution)/shard_map/all_gather | solution.py:25
  153.1 44.2 %reduce-scatter.15.cloned.1.call-start = ((), (), s32[]{:S(2)}) async-start(), calls=%async_computation.11 | async-start | bytes 1310720
  158.3 66.2 %reduce-scatter.13.cloned.1.call-start = ((), (), s32[]{:S(2)}) async-start(), calls=%async_computation.10 | async-start | bytes 1310720
  162.4 7.8 %copy-start.5 = (bf16[2,512,1024]{2,1,0:T(8,128)(2,1)S(1)}, bf16[2,512,1024]{2,1,0:T(8,128)(2,1)}, u32[]{:S(2)}) copy-start(bf16[2,512,1024]{2,1,0:T(8,128)(2,1)} %param.14) | copy-start | bytes 6291460
  174.0 73.8 %all-to-all-start.3 = ((bf16[8,128,1024]{2,1,0:T(8,128)(2,1)}), bf16[8,128,1024]{2,1,0:T(8,128)(2,1)S(1)}, u32[]{:S(2)}, u32[]{:S(2)}) async-start(bf16[8,128,1024]{2,1,0:T(8,128)(2,1)} %convolution_convert_fusion), calls=%async_computation.3 | async-start | bytes 4194304 | tf_op jit(solution)/shard_map/all_to_all | solution.py:32
  179.5 64.2 %all-gather.3.cloned.1.call-start = ((), (), s32[]{:S(2)}) async-start(), calls=%async_computation.8 | async-start | bytes 1310720 | tf_op jit(solution)/shard_map/all_gather | solution.py:25
  247.7 6.0 %copy-start.3 = (f32[512,2]{0,1:T(2,128)S(1)}, f32[512,2]{0,1:T(2,128)}, u32[]{:S(2)}) copy-start(f32[512,2]{0,1:T(2,128)} %param.10) | copy-start | bytes 12292
  247.7 54.4 %all-to-all-start.1 = ((bf16[8,128,1024]{2,1,0:T(8,128)(2,1)}), bf16[8,128,1024]{2,1,0:T(8,128)(2,1)}, u32[]{:S(2)}, u32[]{:S(2)}) async-start(bf16[8,128,1024]{2,1,0:T(8,128)(2,1)} %convolution_convert_fusion.1), calls=%async_computation.1 | async-start | bytes 4194304 | tf_op jit(solution)/shard_map/all_to_all | solution.py:32
  317.4 6.6 %copy-start.2 = (f32[1024]{0:T(1024)S(1)}, f32[1024]{0:T(1024)}, u32[]{:S(2)}) copy-start(f32[1024]{0:T(1024)} %param.15) | copy-start | bytes 12292
Sparse Core Ops, SparseCore 0:
  99.7 23.8 reduce-scatter.18
  126.1 24.8 reduce-scatter.16
  153.3 16.8 all-gather.4
  172.5 24.7 reduce-scatter.14
  199.7 24.7 reduce-scatter.12
  226.8 16.8 all-gather.2
where the time goes:
time: 333 us; the launch traced here: 332 us
  waiting for transfers between devices  155 us (47%)
  blocking collectives  67.1 us (20%)
  local copies, waits for them, and re-layouts  48.2 us (14%)
  matrix products  19.9 us (6%)
  starting transfers between devices  15.9 us (5%)
  between operations  13.8 us (4%)
  other arithmetic  12.8 us (4%)
    unnamed x10, waiting for transfers between devices  82.9 us
    all_to_all x1, blocking collectives, body(): lax.all_to_all(outgoing[:, member], 'ep', split_axis=0, concat_axis=0, ti...  52.7 us
    all_to_all x2, waiting for transfers between devices, serve_single(): lax.all_to_all(expert_rows(weights, block), 'ep', split_axis=0, concat_ax...  48.4 us
    all_gather x2, waiting for transfers between devices, expert_rows(): hidden = lax.all_gather(share, 'tp', axis=2, tiled=True)  23.4 us
    unnamed x29, local copies, waits for them, and re-layouts  15.8 us
    all_to_all x2, starting transfers between devices, serve_single(): lax.all_to_all(expert_rows(weights, block), 'ep', split_axis=0, concat_ax...  11.2 us
    gather x2, local copies, waits for them, and re-layouts, body(): returned[position[:, which]].astype(jnp.float32)  10.9 us
    gather x1, local copies, waits for them, and re-layouts, body(): padded[table].reshape(ep_count, local_count, capacity, normed.shape[1])  9.7 us
  transfers between devices with their start and end apart: 9, of which 7 were waited for; matrix products, arithmetic and copies ran while one was open for 10% of the time, Pallas kernels for 0%

commit v1 on v0

v1 whole, which is shorter than its diff:
```python
import functools

import jax
import jax.numpy as jnp
from jax import lax
from jax.experimental import pallas as pl
from jax.experimental.pallas import tpu as pltpu
from jax.sharding import PartitionSpec as P

EPSILON = 1e-06
BF = jnp.bfloat16
F32 = jnp.float32


def dot(a, b):
    return jnp.dot(a, b, preferred_element_type=F32)


def dot_t(a, b):
    return lax.dot_general(a, b, (((0,), (0,)), ((), ())), preferred_element_type=F32)


def kernel(
    n, nt, local, cap,
    x_ref, rank_ref, wt_ref, gate_hbm, up_hbm, down_hbm, out_ref,
    gate_v, up_v, down_v, send_x, recv_x, part, recv_p, hid, out_s, out_r,
    w_sem, xs_sem, xr_sem, ps_sem, pr_sem, hs_sem, hr_sem, os_sem, or_sem,
):
    me = lax.axis_index("ep")
    my_tp = lax.axis_index("tp")
    ff = gate_v.shape[2]
    fq = ff // nt

    loads = [
        pltpu.make_async_copy(src, dst, w_sem.at[i])
        for i, (src, dst) in enumerate(((gate_hbm, gate_v), (up_hbm, up_v), (down_hbm, down_v)))
    ]
    for load in loads:
        load.start()

    barrier = pltpu.get_barrier_semaphore()

    @pl.loop(1, n)
    def _(s):
        pl.semaphore_signal(barrier, inc=1, device_id={"ep": lax.rem(me + s, n), "tp": my_tp})

    for o in range(1, nt):
        pl.semaphore_signal(barrier, inc=1, device_id={"ep": me, "tp": lax.rem(my_tp + o, nt)})

    def onehot(owner, weighted):
        rows = []
        for j in range(local):
            rank = rank_ref[owner * local + j]
            hit = lax.broadcasted_iota(jnp.int32, (cap, rank.shape[1]), 0) == rank
            value = wt_ref[owner * local + j] if weighted else F32(1.0)
            rows.append(jnp.where(hit, value, F32(0.0)))
        return jnp.concatenate(rows, axis=0)

    def pack(owner):
        return dot(onehot(owner, False).astype(BF), x_ref[...]).astype(BF)

    def dest(s):
        return lax.rem(me + s, n)

    def source(s):
        return lax.rem(me - s + n, n)

    def x_copy(s):
        d = dest(s)
        return pltpu.make_async_remote_copy(
            send_x.at[d], recv_x.at[me], xs_sem.at[d], xr_sem.at[me],
            device_id={"ep": d, "tp": my_tp},
        )

    def x_arrival(s):
        b = source(s)
        return pltpu.make_async_remote_copy(
            send_x.at[b], recv_x.at[b], xs_sem.at[b], xr_sem.at[b],
            device_id={"ep": b, "tp": my_tp},
        )

    def p_copy(s, o):
        b = source(s)
        q = lax.rem(my_tp + o, nt)
        return pltpu.make_async_remote_copy(
            part.at[b, q], recv_p.at[b, o - 1], ps_sem.at[b, o - 1], pr_sem.at[b, o - 1],
            device_id={"ep": me, "tp": q},
        )

    def h_copy(s, o):
        b = source(s)
        q = lax.rem(my_tp + o, nt)
        return pltpu.make_async_remote_copy(
            hid.at[b, my_tp], hid.at[b, my_tp], hs_sem.at[b, o - 1], hr_sem.at[b, o - 1],
            device_id={"ep": me, "tp": q},
        )

    def h_arrival(s, o):
        b = source(s)
        q = lax.rem(my_tp - o + nt, nt)
        return pltpu.make_async_remote_copy(
            hid.at[b, q], hid.at[b, q], hs_sem.at[b, o - 1], hr_sem.at[b, o - 1],
            device_id={"ep": me, "tp": q},
        )

    def o_copy(s):
        b = source(s)
        return pltpu.make_async_remote_copy(
            out_s.at[b], out_r.at[me], os_sem.at[b], or_sem.at[me],
            device_id={"ep": b, "tp": my_tp},
        )

    def o_arrival(s):
        d = dest(s)
        return pltpu.make_async_remote_copy(
            out_s.at[d], out_r.at[d], os_sem.at[d], or_sem.at[d],
            device_id={"ep": d, "tp": my_tp},
        )

    def stage_a(s):
        b = source(s)
        for j in range(local):
            rows = recv_x[b, pl.ds(j * cap, cap), :]
            gate = dot(rows, gate_v[j]).astype(BF)
            upper = dot(rows, up_v[j]).astype(BF)
            for q in range(nt):
                part[b, q, pl.ds(j * cap, cap), pl.ds(0, fq)] = gate[:, q * fq:(q + 1) * fq]
                part[b, q, pl.ds(j * cap, cap), pl.ds(fq, fq)] = upper[:, q * fq:(q + 1) * fq]
        for o in range(1, nt):
            p_copy(s, o).start()

    def stage_b(s):
        b = source(s)
        for o in range(1, nt):
            p_copy(s, o).wait_recv()
        total = part[b, my_tp].astype(F32)
        for o in range(1, nt):
            total = total + recv_p[b, o - 1].astype(F32)
        gate, upper = total[:, :fq], total[:, fq:]
        hid[b, my_tp] = (gate / (1.0 + jnp.exp(-gate)) * upper).astype(BF)
        for o in range(1, nt):
            h_copy(s, o).start()

    def stage_c(s, own):
        b = source(s)
        for o in range(1, nt):
            h_arrival(s, o).wait_recv()
        for j in range(local):
            hidden = jnp.concatenate([hid[b, q, pl.ds(j * cap, cap), :] for q in range(nt)], axis=1)
            result = dot(hidden, down_v[j]).astype(BF)
            if own:
                out_r[me, pl.ds(j * cap, cap), :] = result
            else:
                out_s[b, pl.ds(j * cap, cap), :] = result
        if not own:
            o_copy(s).start()

    def combine(s):
        d = dest(s)
        weight = onehot(d, True)
        high = weight.astype(BF)
        low = (weight - high.astype(F32)).astype(BF)
        rows = out_r[d]
        return dot_t(high, rows) + dot_t(low, rows)

    send_x[dest(1)] = pack(dest(1))
    pl.semaphore_wait(barrier, n - 1 + nt - 1)

    @pl.loop(2, n)
    def _(s):
        send_x[dest(s)] = pack(dest(s))
        x_copy(s - 1).start()

    recv_x[me] = pack(me)
    x_copy(n - 1).start()

    for load in loads:
        load.wait()
    stage_a(0)
    x_arrival(1).wait_recv()
    stage_a(1)
    stage_b(0)
    x_arrival(2).wait_recv()
    stage_a(2)
    stage_b(1)
    stage_c(0, True)
    out_ref[...] = combine(0)

    @pl.loop(3, n)
    def _(s):
        x_arrival(s).wait_recv()
        stage_a(s)
        stage_b(s - 1)
        stage_c(s - 2, False)

    stage_b(n - 1)
    stage_c(n - 2, False)
    stage_c(n - 1, False)

    @pl.loop(1, n)
    def _(s):
        o_arrival(s).wait_recv()
        out_ref[...] += combine(s)

    @pl.loop(0, n)
    def _(s):
        for o in range(1, nt):
            p_copy(s, o).wait_send()
            h_copy(s, o).wait_send()

    @pl.loop(1, n)
    def _(s):
        x_copy(s).wait_send()
        o_copy(s).wait_send()


def body(tokens, routes, route_weights, norm_gain, gate_weight, up_weight, down_weight, final_gain):
    n, nt = lax.axis_size("ep"), lax.axis_size("tp")
    local, width, ff = gate_weight.shape
    experts = n * local
    rows = tokens.shape[0]
    full = width * nt
    cap = 4 * rows // experts
    count = local * cap
    values = tokens.astype(F32)
    squares = lax.psum(jnp.sum(values * values, axis=-1), "tp")
    normed = (values * lax.rsqrt(squares / full + EPSILON)[:, None] * norm_gain).astype(BF)
    names = jnp.arange(experts, dtype=jnp.int32)[:, None, None]
    match = routes.T[None, :, :] == names
    hit = jnp.any(match, axis=1)
    weight = jnp.sum(jnp.where(match, route_weights.T[None], 0.0), axis=1)
    steps = jnp.arange(rows, dtype=jnp.int32)
    earlier = (steps[:, None] < steps[None, :]).astype(BF)
    before = dot(hit.astype(BF), earlier).astype(jnp.int32)
    rank = jnp.where(hit, before, -1)

    any_spec = pl.BlockSpec(memory_space=pl.ANY)
    vmem = pl.BlockSpec(memory_space=pltpu.VMEM)
    dma = pltpu.SemaphoreType.DMA
    combined = pl.pallas_call(
        functools.partial(kernel, n, nt, local, cap),
        out_shape=jax.ShapeDtypeStruct((rows, width), F32),
        in_specs=[vmem, vmem, vmem, any_spec, any_spec, any_spec],
        out_specs=vmem,
        scratch_shapes=[
            pltpu.VMEM(gate_weight.shape, BF),
            pltpu.VMEM(up_weight.shape, BF),
            pltpu.VMEM(down_weight.shape, BF),
            pltpu.VMEM((n, count, width), BF),
            pltpu.VMEM((n, count, width), BF),
            pltpu.VMEM((n, nt, count, 2 * ff // nt), BF),
            pltpu.VMEM((n, nt - 1, count, 2 * ff // nt), BF),
            pltpu.VMEM((n, nt, count, ff // nt), BF),
            pltpu.VMEM((n, count, width), BF),
            pltpu.VMEM((n, count, width), BF),
            dma((3,)),
            dma((n,)),
            dma((n,)),
            dma((n, nt - 1)),
            dma((n, nt - 1)),
            dma((n, nt - 1)),
            dma((n, nt - 1)),
            dma((n,)),
            dma((n,)),
        ],
        compiler_params=pltpu.CompilerParams(
            collective_id=0, has_side_effects=True, vmem_limit_bytes=60 * 1024 * 1024
        ),
    )(normed, rank[:, None, :], weight[:, None, :], gate_weight, up_weight, down_weight)
    closing = lax.psum(jnp.sum(combined * combined, axis=-1), "tp")
    return (combined * lax.rsqrt(closing / full + EPSILON)[:, None] * final_gain).astype(BF)


def solution(mesh):
    in_specs = (
        P("ep", "tp"),
        P("ep", None),
        P("ep", None),
        P("tp"),
        P("ep", "tp", None),
        P("ep", "tp", None),
        P("ep", None, "tp"),
        P("tp"),
    )
    return jax.shard_map(body, mesh=mesh, in_specs=in_specs, out_specs=P("ep", "tp"), check_vma=False)
```

time: 333 us -> 255 us (0.77)
  Pallas kernels: 0 us -> 230 us
  waiting for transfers between devices: 155 us -> 0 us
  blocking collectives: 67.1 us -> 15 us
  local copies, waits for them, and re-layouts: 48.2 us -> 1.28 us
  matrix products: 19.9 us -> 0.18 us
  starting transfers between devices: 15.9 us -> 0 us
  between operations: 13.8 us -> 0.04 us
  other arithmetic: 12.8 us -> 8.16 us
    pallas_call x0 -> x1, Pallas kernels: none -> 230 us  [body(): pl.pallas_call(functools.partial(kernel, n, nt, local, cap), out_shape=ja...]
    unnamed x10 -> x0, waiting for transfers between devices: 82.9 us -> none
    all_to_all x1 -> x0, blocking collectives: 52.7 us -> none  [body(): lax.all_to_all(outgoing[:, member], 'ep', split_axis=0, concat_axis=0, ti...]
    all_to_all x3 -> x0, waiting for transfers between devices: 48.4 us -> none  [the longest x2 48.4 us: serve_single(): lax.all_to_all(expert_rows(weights, block), 'ep', split_axis=0, concat_ax...]
    all_gather x2 -> x0, waiting for transfers between devices: 23.4 us -> none  [expert_rows(): hidden = lax.all_gather(share, 'tp', axis=2, tiled=True)]
    gather x3 -> x0, local copies, waits for them, and re-layouts: 20.6 us -> none  [the longest x2 10.9 us: body(): returned[position[:, which]].astype(jnp.float32)]
    dot_general x6 -> x1, matrix products: 19.9 us -> 0.18 us  [dot(): return jnp.dot(a, b, preferred_element_type=F32)]
    unnamed x29 -> x6, local copies, waits for them, and re-layouts: 15.8 us -> 0.01 us
  transfers between devices with their start and end apart: 9 -> 0, of which waited for: 7 -> 0; matrix products, arithmetic and copies ran while one was open for 10% -> 0% of each run, Pallas kernels for 0% -> 0%
where the time goes in v1:
time: 255 us; the launch traced here: 254 us
  Pallas kernels  230 us (90%)
  blocking collectives  15 us (6%)
  other arithmetic  8.16 us (3%)
    pallas_call x1, Pallas kernels, body(): pl.pallas_call(functools.partial(kernel, n, nt, local, cap), out_shape=ja...  230 us
    psum x1, blocking collectives, body(): squares = lax.psum(jnp.sum(values * values, axis=-1), 'tp')  8.4 us
    psum x1, blocking collectives, body(): closing = lax.psum(jnp.sum(combined * combined, axis=-1), 'tp')  6.64 us

profile of v1, /device:TPU:0, one launch (start us, length us, event | category | flops | bytes accessed | tf_op | source)
XLA Modules:
  0.0 254.4 jit_solution(15129166668034354083)
XLA Ops:
  0.0 0.0 copy-start.1
  0.0 1.6 fusion
  1.6 8.4 %psum.14 = f32[512]{0:T(512)S(1)} all-reduce(f32[512]{0:T(512)S(1)} %fusion), channel_id=1, replica_groups=mesh['ep'=8,'tp'=4] {'tp'}, use_global_device_ids=true, to_apply=%region_1.0 | all-reduce | flops 512 | bytes 4096 | tf_op jit(solution)/shard_map/psum | solution.py:226
  10.0 0.7 fusion.4
  10.7 0.2 fusion.3
  10.9 0.6 broadcast_in_dim.32.rank_ref
  11.5 0.7 select_reduce_fusion
  12.2 0.6 broadcast_in_dim.35.wt_ref
  12.9 0.0 copy-done.1
  12.9 2.0 fusion.2.x_ref
  14.8 229.8 %shard_map.82 = f32[512,1024]{1,0:T(8,128)} custom-call(bf16[512,1024]{1,0:T(8,128)(2,1)} %fusion.2.x_ref, s32[16,1,512]{2,1,0:T(1,128)} %broadcast_in_dim.32.rank_ref, f32[16,1,512]{2,1,0:T(1,128)} %broadcast_in_dim.35.wt_ref, bf16[2,1024,512]{2,1,0:T(8,128)(2,1)} %gate_hbm.1, bf16[2,1024,512]{2,1,0:T(8,128)(2,1)} %up_hbm.1, bf16[2,512,1024]{2,1,0:T(8,128)(2,1)} %down_hbm.1), custom_call_target="tpu_custom_call" | custom-call | tf_op jit(solution)/shard_map/pallas_call | solution.py:240
  244.6 0.0 copy-start
  244.6 0.0 copy-start.2
  244.6 1.9 multiply_reduce_fusion
  246.6 6.6 %psum.15 = f32[512]{0:T(512)S(1)} all-reduce(f32[512]{0:T(512)S(1)} %multiply_reduce_fusion), channel_id=1, replica_groups=mesh['ep'=8,'tp'=4] {'tp'}, use_global_device_ids=true, to_apply=%region_5.6 | all-reduce | flops 512 | bytes 4096 | tf_op jit(solution)/shard_map/psum | solution.py:270
  253.2 0.0 copy-done
  253.2 0.0 copy-done.2
  253.2 1.2 multiply_convert_fusion
  (2 shorter events, 0.0 us)
Async XLA Ops:
  0.0 12.9 %copy-start.1 = (bf16[512,1024]{1,0:T(8,128)(2,1)S(1)}, bf16[512,1024]{1,0:T(8,128)(2,1)}, u32[]{:S(2)}) copy-start(bf16[512,1024]{1,0:T(8,128)(2,1)} %param.8) | copy-start | bytes 3145732
  244.6 8.6 %copy-start = (f32[512,1024]{1,0:T(8,128)S(1)}, f32[512,1024]{1,0:T(8,128)}, u32[]{:S(2)}) copy-start(f32[512,1024]{1,0:T(8,128)} %shard_map.82) | copy-start | bytes 6291460
  244.6 8.6 %copy-start.2 = (f32[1024]{0:T(1024)S(1)}, f32[1024]{0:T(1024)}, u32[]{:S(2)}) copy-start(f32[1024]{0:T(1024)} %param.15) | copy-start | bytes 12292

commit v2 on v1

v2 whole, which is shorter than its diff:
```python
import functools

import jax
import jax.numpy as jnp
from jax import lax
from jax.experimental import pallas as pl
from jax.experimental.pallas import tpu as pltpu
from jax.sharding import PartitionSpec as P

EPSILON = 1e-06
BF = jnp.bfloat16
F32 = jnp.float32


def dot(a, b):
    return jnp.dot(a, b, preferred_element_type=F32)


def dot_t(a, b):
    return lax.dot_general(a, b, (((0,), (0,)), ((), ())), preferred_element_type=F32)


def kernel(
    n, nt, local, cap, ring, full,
    x_ref, meta_ref, gain_ref, last_gain_ref, gate_hbm, up_hbm, down_hbm, out_ref,
    gate_v, up_v, down_v, xn, acc, tri, rank_t, wt_t, sq, sq2,
    send_x, recv_x, pk_s, pk_r, far_r, meta_r,
    part, recv_p, hid, out_s, out_r,
    w_sem, xs_sem, xr_sem, ks_sem, kr_sem, fs_sem, fr_sem, ms_sem, mr_sem,
    ps_sem, pr_sem, hs_sem, hr_sem, os_sem, or_sem, qs_sem, qr_sem,
):
    me = lax.axis_index("ep")
    my_tp = lax.axis_index("tp")
    ff = gate_v.shape[2]
    fq = ff // nt
    rows_all = x_ref.shape[0]
    half = n // 2
    chunk = rows_all // 2
    count = local * cap
    split = local // 2

    loads = [
        pltpu.make_async_copy(src, dst, w_sem.at[i])
        for i, (src, dst) in enumerate(((gate_hbm, gate_v), (up_hbm, up_v), (down_hbm, down_v)))
    ]
    for load in loads:
        load.start()

    barrier = pltpu.get_barrier_semaphore()

    @pl.loop(1, n)
    def _(s):
        pl.semaphore_signal(barrier, inc=1, device_id={"ep": lax.rem(me + s, n), "tp": my_tp})

    for o in range(1, nt):
        pl.semaphore_signal(barrier, inc=1, device_id={"ep": me, "tp": lax.rem(my_tp + o, nt)})

    place = jnp.where(me % 2 == 0, me // 2, n - 1 - me // 2)

    def at_place(p):
        p = lax.rem(p + 2 * n, n)
        return jnp.where(p < half, 2 * p, 2 * (n - 1 - p) + 1)

    def shift(s):
        return (1 - 2 * ((s + 1) % 2)) * ((s + 1) // 2)

    def source(s):
        if ring:
            return at_place(place - shift(s))
        return lax.rem(me - s + n, n)

    def sender(s):
        if ring:
            return at_place(place + shift(s))
        return lax.rem(me + s, n)

    def eye():
        shape = (rows_all, rows_all)
        return lax.broadcasted_iota(jnp.int32, shape, 0) == lax.broadcasted_iota(jnp.int32, shape, 1)

    def sq_copy(k, o):
        q = lax.rem(my_tp + o, nt)
        return pltpu.make_async_remote_copy(
            sq.at[k], sq2.at[k, o - 1], qs_sem.at[k, o - 1], qr_sem.at[k, o - 1],
            device_id={"ep": me, "tp": q},
        )

    def start_sum(k, column):
        row = jnp.sum(jnp.where(eye(), column, 0.0), axis=0, keepdims=True)
        sq[k] = jnp.broadcast_to(row, sq.shape[1:])

    def send_sum(k):
        for o in range(1, nt):
            sq_copy(k, o).start()

    def finish_sum(k):
        for o in range(1, nt):
            sq_copy(k, o).wait_recv()
        total = sq[k]
        for o in range(1, nt):
            total = total + sq2[k, o - 1]
        scale = lax.rsqrt(total[0:1] / full + EPSILON)
        return jnp.sum(jnp.where(eye(), scale, 0.0), axis=1, keepdims=True)

    def make_table(slot, meta):
        names = lax.broadcasted_iota(jnp.int32, rank_t.shape[1:], 0).astype(F32)
        first, second = meta[0:1] == names, meta[1:2] == names
        hit = first | second
        before = dot(jnp.where(hit, 1.0, 0.0).astype(BF), tri[...])
        rank_t[slot] = jnp.where(hit, before, -1.0)
        wt_t[slot] = jnp.where(first, meta[2:3], 0.0) + jnp.where(second, meta[3:4], 0.0)

    def onehot(slot, expert, weighted=False):
        rank = rank_t[slot, pl.ds(expert, 1), :]
        hit = lax.broadcasted_iota(jnp.int32, (cap, rows_all), 0).astype(F32) == rank
        return jnp.where(hit, wt_t[slot, pl.ds(expert, 1), :] if weighted else F32(1.0), F32(0.0))

    def pack(slot, experts, block):
        pick = jnp.concatenate([onehot(slot, e) for e in experts], axis=0).astype(BF)
        return dot(pick, block).astype(BF)

    def experts_of(owner):
        return [owner * local + j for j in range(local)]

    def x_copy(s):
        return pltpu.make_async_remote_copy(
            send_x.at[s], recv_x.at[s], xs_sem.at[s], xr_sem.at[s],
            device_id={"ep": sender(s), "tp": my_tp},
        )

    def ahead(i):
        return {"ep": at_place(place + 1 - 2 * i), "tp": my_tp}

    def block_copy(d, i, k):
        piece = pl.ds(k * chunk, chunk)
        src = xn.at[piece] if d == 1 else recv_x.at[2 * d - 4 + i, piece]
        slot = 2 * d - 2 + i
        return pltpu.make_async_remote_copy(
            src, recv_x.at[slot, piece], xs_sem.at[slot, k], xr_sem.at[slot, k], device_id=ahead(i)
        )

    def meta_copy(d, i):
        slot = 2 * d - 2 + i
        return pltpu.make_async_remote_copy(
            meta_ref if d == 1 else meta_r.at[slot - 2], meta_r.at[slot],
            ms_sem.at[slot], mr_sem.at[slot], device_id=ahead(i),
        )

    def pack_copy(i):
        return pltpu.make_async_remote_copy(
            pk_s.at[i], pk_r.at[i], ks_sem.at[i], kr_sem.at[i], device_id=ahead(i)
        )

    def far_copy(i):
        return pltpu.make_async_remote_copy(
            pk_r.at[i, pl.ds(count, split * cap)], far_r.at[i], fs_sem.at[i], fr_sem.at[i],
            device_id=ahead(i),
        )

    def p_copy(s, o):
        q = lax.rem(my_tp + o, nt)
        return pltpu.make_async_remote_copy(
            part.at[s, q], recv_p.at[s, o - 1], ps_sem.at[s, o - 1], pr_sem.at[s, o - 1],
            device_id={"ep": me, "tp": q},
        )

    def h_copy(s, o, back=False):
        mine = lax.rem(my_tp - o + nt, nt) if back else my_tp
        q = lax.rem(my_tp - o + nt, nt) if back else lax.rem(my_tp + o, nt)
        return pltpu.make_async_remote_copy(
            hid.at[s, mine], hid.at[s, mine], hs_sem.at[s, o - 1], hr_sem.at[s, o - 1],
            device_id={"ep": me, "tp": q},
        )

    def o_copy(s):
        return pltpu.make_async_remote_copy(
            out_s.at[s], out_r.at[s], os_sem.at[s], or_sem.at[s],
            device_id={"ep": source(s), "tp": my_tp},
        )

    def stage_a(s, rows_of):
        for j in range(local):
            rows = rows_of(j)
            gate = dot(rows, gate_v[j]).astype(BF)
            upper = dot(rows, up_v[j]).astype(BF)
            for q in range(nt):
                part[s, q, pl.ds(j * cap, cap), pl.ds(0, fq)] = gate[:, q * fq:(q + 1) * fq]
                part[s, q, pl.ds(j * cap, cap), pl.ds(fq, fq)] = upper[:, q * fq:(q + 1) * fq]
        for o in range(1, nt):
            p_copy(s, o).start()

    def stage_b(s):
        for o in range(1, nt):
            p_copy(s, o).wait_recv()
        total = part[s, my_tp].astype(F32)
        for o in range(1, nt):
            total = total + recv_p[s, o - 1].astype(F32)
        gate, upper = total[:, :fq], total[:, fq:]
        hid[s, my_tp] = (gate / (1.0 + jnp.exp(-gate)) * upper).astype(BF)
        for o in range(1, nt):
            h_copy(s, o).start()

    def stage_c(s, own):
        for o in range(1, nt):
            h_copy(s, o, True).wait_recv()
        target = out_r if own else out_s
        for j in range(local):
            hidden = jnp.concatenate([hid[s, q, pl.ds(j * cap, cap), :] for q in range(nt)], axis=1)
            target[s, pl.ds(j * cap, cap), :] = dot(hidden, down_v[j]).astype(BF)
        if not own:
            o_copy(s).start()

    def combine(s):
        weight = jnp.concatenate([onehot(0, e, True) for e in experts_of(sender(s))], axis=0)
        high = weight.astype(BF)
        low = (weight - high.astype(F32)).astype(BF)
        rows = out_r[s]
        return dot_t(high, rows) + dot_t(low, rows)

    values = x_ref[...].astype(F32)
    start_sum(0, jnp.sum(values * values, axis=1, keepdims=True))
    shape = (rows_all, rows_all)
    earlier = lax.broadcasted_iota(jnp.int32, shape, 0) < lax.broadcasted_iota(jnp.int32, shape, 1)
    tri[...] = jnp.where(earlier, 1.0, 0.0).astype(BF)
    pl.semaphore_wait(barrier, n - 1 + nt - 1)
    send_sum(0)
    if ring:
        for i in range(2):
            meta_copy(1, i).start()
    make_table(0, meta_ref[...])
    scale = finish_sum(0)
    xn[...] = (x_ref[...].astype(F32) * scale * gain_ref[...]).astype(BF)

    def own_rows(j):
        return pack(0, [me * local + j], xn[...])

    def stored(ref, slot):
        return lambda j: ref[slot, pl.ds(j * cap, cap), :]

    if ring:
        for k in range(2):
            for i in range(2):
                block_copy(1, i, k).start()
        for load in loads:
            load.wait()
        stage_a(0, own_rows)
        for d in range(1, half + 1):
            if d <= half - 2:
                for k in range(2):
                    for i in range(2):
                        block_copy(d, i, k).wait_recv()
                        if d < half - 2:
                            block_copy(d + 1, i, k).start()
                for i in range(2):
                    slot = 2 * d - 2 + i
                    meta_copy(d, i).wait_recv()
                    if d < half - 2:
                        meta_copy(d + 1, i).start()
                    make_table(1 + slot, meta_r[slot])
                if d == half - 2:
                    for i in range(2):
                        slot = 2 * d - 2 + i
                        step = 1 - 2 * i
                        far = experts_of(at_place(place + 2 * step))
                        wanted = experts_of(at_place(place + step)) + (far[split:] if i else far[:split])
                        pk_s[i] = pack(1 + slot, wanted, recv_x[slot])
                        pack_copy(i).start()
            elif d == half - 1:
                for i in range(2):
                    pack_copy(i).wait_recv()
                    far_copy(i).start()
            else:
                for i in range(2):
                    far_copy(i).wait_recv()
            for i in range(2 if d < half else 1):
                s = 2 * d - 1 + i
                slot = s - 1
                if d <= half - 2:
                    stage_a(s, lambda j, slot=slot: pack(1 + slot, [me * local + j], recv_x[slot]))
                elif d == half - 1:
                    stage_a(s, stored(pk_r, i))
                else:
                    stage_a(s, lambda j: far_r[j // split, pl.ds(j % split * cap, cap), :])
                stage_b(s - 1)
                if s >= 2:
                    stage_c(s - 2, s == 2)
    else:
        send_x[1] = pack(0, experts_of(sender(1)), xn[...])

        @pl.loop(2, n)
        def _(s):
            send_x[s] = pack(0, experts_of(sender(s)), xn[...])
            x_copy(s - 1).start()

        for load in loads:
            load.wait()
        stage_a(0, own_rows)
        x_copy(n - 1).start()
        x_copy(1).wait_recv()
        stage_a(1, stored(recv_x, 1))
        stage_b(0)
        x_copy(2).wait_recv()
        stage_a(2, stored(recv_x, 2))
        stage_b(1)
        stage_c(0, True)

        @pl.loop(3, n)
        def _(s):
            x_copy(s).wait_recv()
            stage_a(s, stored(recv_x, s))
            stage_b(s - 1)
            stage_c(s - 2, False)

    stage_b(n - 1)
    stage_c(n - 2, False)
    acc[...] = combine(0)
    stage_c(n - 1, False)

    @pl.loop(1, n)
    def _(s):
        o_copy(s).wait_recv()
        acc[...] += combine(s)

    summed = acc[...]
    start_sum(1, jnp.sum(summed * summed, axis=1, keepdims=True))

    @pl.loop(0, n)
    def _(s):
        for o in range(1, nt):
            p_copy(s, o).wait_send()
            h_copy(s, o).wait_send()

    send_sum(1)

    @pl.loop(1, n)
    def _(s):
        o_copy(s).wait_send()

    if ring:
        for i in range(2):
            for d in range(1, half - 1):
                meta_copy(d, i).wait_send()
                for k in range(2):
                    block_copy(d, i, k).wait_send()
            pack_copy(i).wait_send()
            far_copy(i).wait_send()
    else:
        @pl.loop(1, n)
        def _(s):
            x_copy(s).wait_send()

    scale = finish_sum(1)
    out_ref[...] = (acc[...] * scale * last_gain_ref[...]).astype(BF)
    for k in range(2):
        for o in range(1, nt):
            sq_copy(k, o).wait_send()


RING_BYTES = 24 * 1024 * 1024


def body(tokens, routes, route_weights, norm_gain, gate_weight, up_weight, down_weight, final_gain):
    n, nt = lax.axis_size("ep"), lax.axis_size("tp")
    local, width, ff = gate_weight.shape
    experts = n * local
    rows = tokens.shape[0]
    full = width * nt
    cap = 4 * rows // experts
    count = local * cap
    blocks = max(n - 4, 0)
    ring = n % 2 == 0 and n >= 6 and local % 2 == 0 and blocks * rows * width * 2 <= RING_BYTES
    meta = jnp.concatenate(
        [routes.T.astype(F32), route_weights.T, jnp.zeros((4, rows), F32)], axis=0
    )
    tables = 1 + blocks if ring else 1
    packed = count + local // 2 * cap

    any_spec = pl.BlockSpec(memory_space=pl.ANY)
    vmem = pl.BlockSpec(memory_space=pltpu.VMEM)
    dma = pltpu.SemaphoreType.DMA

    def only(ring_shape, shape, kind=BF):
        return pltpu.VMEM(ring_shape if ring else shape, kind)

    tiny = (1, 16, 128)
    return pl.pallas_call(
        functools.partial(kernel, n, nt, local, cap, ring, full),
        out_shape=jax.ShapeDtypeStruct((rows, width), BF),
        in_specs=[vmem, vmem, vmem, vmem, any_spec, any_spec, any_spec],
        out_specs=vmem,
        scratch_shapes=[
            pltpu.VMEM(gate_weight.shape, BF),
            pltpu.VMEM(up_weight.shape, BF),
            pltpu.VMEM(down_weight.shape, BF),
            pltpu.VMEM((rows, width), BF),
            pltpu.VMEM((rows, width), F32),
            pltpu.VMEM((rows, rows), BF),
            pltpu.VMEM((tables, experts, rows), F32),
            pltpu.VMEM((tables, experts, rows), F32),
            pltpu.VMEM((2, 8, rows), F32),
            pltpu.VMEM((2, nt - 1, 8, rows), F32),
            only(tiny, (n, count, width)),
            only((blocks, rows, width), (n, count, width)),
            only((2, packed, width), tiny),
            only((2, packed, width), tiny),
            only((2, local // 2 * cap, width), tiny),
            only((blocks, 8, rows), (1, 8, 128), F32),
            pltpu.VMEM((n, nt, count, 2 * ff // nt), BF),
            pltpu.VMEM((n, nt - 1, count, 2 * ff // nt), BF),
            pltpu.VMEM((n, nt, count, ff // nt), BF),
            pltpu.VMEM((n, count, width), BF),
            pltpu.VMEM((n, count, width), BF),
            dma((3,)),
            dma((blocks, 2) if ring else (n,)),
            dma((blocks, 2) if ring else (n,)),
            dma((2,)),
            dma((2,)),
            dma((2,)),
            dma((2,)),
            dma((blocks,) if ring else (1,)),
            dma((blocks,) if ring else (1,)),
            dma((n, nt - 1)),
            dma((n, nt - 1)),
            dma((n, nt - 1)),
            dma((n, nt - 1)),
            dma((n,)),
            dma((n,)),
            dma((2, nt - 1)),
            dma((2, nt - 1)),
        ],
        compiler_params=pltpu.CompilerParams(
            collective_id=0, has_side_effects=True, vmem_limit_bytes=60 * 1024 * 1024
        ),
    )(tokens, meta, norm_gain[None], final_gain[None], gate_weight, up_weight, down_weight)


def solution(mesh):
    in_specs = (
        P("ep", "tp"),
        P("ep", None),
        P("ep", None),
        P("tp"),
        P("ep", "tp", None),
        P("ep", "tp", None),
        P("ep", None, "tp"),
        P("tp"),
    )
    return jax.shard_map(body, mesh=mesh, in_specs=in_specs, out_specs=P("ep", "tp"), check_vma=False)
```

time: 255 us -> 182 us (0.71)
  the two profiles are of different devices: /device:TPU:0 before, /device:TPU:11 now
where the time goes in v2:
time: 182 us
  Pallas kernels  177 us (97%)
  local copies, waits for them, and re-layouts  2.34 us (1%)
  other arithmetic  2.05 us (1%)
    pallas_call x1, Pallas kernels, body(): pl.pallas_call(functools.partial(kernel, n, nt, local, cap, ring, full),...  177 us

profile of v2, /device:TPU:11, one launch (start us, length us, event | category | flops | bytes accessed | tf_op | source)
XLA Modules:
  0.0 181.7 jit_solution(14577639221121656731)
XLA Ops:
  0.0 0.1 pad.2.clone
  0.1 0.7 convert_bitcast_fusion
  0.8 1.4 maximum_maximum_fusion.meta_ref
  2.1 177.3 %shard_map.82 = bf16[512,1024]{1,0:T(8,128)(2,1)} custom-call(bf16[512,1024]{1,0:T(8,128)(2,1)} %x_ref.1, f32[8,512]{1,0:T(8,128)} %maximum_maximum_fusion.meta_ref, f32[1,1024]{1,0:T(1,128)} %bitcast.5, f32[1,1024]{1,0:T(1,128)} %bitcast.6, bf16[2,1024,512]{2,1,0:T(8,128)(2,1)} %gate_hbm.1, bf16[2,1024,512]{2,1,0:T(8,128)(2,1)} %up_hbm.1, ...), custom_call_target="tpu_custom_call" | custom-call | tf_op jit(solution)/shard_map/pallas_call | solution.py:386
  179.5 2.3 %copy.10 = bf16[512,1024]{1,0:T(8,128)(2,1)} copy(bf16[512,1024]{1,0:T(8,128)(2,1)} %shard_map.82) | data formatting | bytes 2097152
  (1 shorter events, 0.0 us)

commit v3 on v2

--- a/solution.py
+++ b/solution.py
@@ -24,10 +24,10 @@
     n, nt, local, cap, ring, full,
     x_ref, meta_ref, gain_ref, last_gain_ref, gate_hbm, up_hbm, down_hbm, out_ref,
     gate_v, up_v, down_v, xn, acc, tri, rank_t, wt_t, sq, sq2,
-    send_x, recv_x, pk_s, pk_r, far_r, meta_r,
-    part, recv_p, hid, out_s, out_r,
+    send_x, recv_x, pk_s, pk_r, far_r, meta_r, meta_a,
+    part, recv_p, hid, out_s, ret, agg_s, agg_r,
     w_sem, xs_sem, xr_sem, ks_sem, kr_sem, fs_sem, fr_sem, ms_sem, mr_sem,
-    ps_sem, pr_sem, hs_sem, hr_sem, os_sem, or_sem, qs_sem, qr_sem,
+    ps_sem, pr_sem, hs_sem, hr_sem, os_sem, or_sem, qs_sem, qr_sem, as_sem, ar_sem,
 ):
     me = lax.axis_index("ep")
     my_tp = lax.axis_index("tp")
@@ -55,7 +55,12 @@
     for o in range(1, nt):
         pl.semaphore_signal(barrier, inc=1, device_id={"ep": me, "tp": lax.rem(my_tp + o, nt)})
 
-    place = jnp.where(me % 2 == 0, me // 2, n - 1 - me // 2)
+    def place_of(index):
+        return jnp.where(index % 2 == 0, index // 2, n - 1 - index // 2)
+
+    place = place_of(me)
+    seat, base = me % half, me // half * half
+    opposite = lax.rem(me + half, n)
 
     def at_place(p):
         p = lax.rem(p + 2 * n, n)
@@ -68,6 +73,12 @@
         if ring:
             return at_place(place - shift(s))
         return lax.rem(me - s + n, n)
+
+    def opposite_step():
+        if not ring:
+            return half
+        delta = lax.rem(place - place_of(opposite) + n, n)
+        return jnp.where(delta <= half, 2 * delta - 1, 2 * (n - delta))
 
     def sender(s):
         if ring:
@@ -172,10 +183,32 @@
             device_id={"ep": me, "tp": q},
         )
 
+    def o_target(s):
+        b = source(s)
+        far = jnp.where(b // half == me // half, 0, 1)
+        return far, jnp.where(far == 0, b, lax.rem(b + half, n))
+
     def o_copy(s):
-        return pltpu.make_async_remote_copy(
-            out_s.at[s], out_r.at[s], os_sem.at[s], or_sem.at[s],
-            device_id={"ep": source(s), "tp": my_tp},
+        far, target = o_target(s)
+        return pltpu.make_async_remote_copy(
+            out_s.at[s], ret.at[far, seat], os_sem.at[s], or_sem.at[far, seat],
+            device_id={"ep": target, "tp": my_tp},
+        )
+
+    def o_arrival(far, other):
+        return pltpu.make_async_remote_copy(
+            out_s.at[0], ret.at[far, other], os_sem.at[0], or_sem.at[far, other],
+            device_id={"ep": base + other, "tp": my_tp},
+        )
+
+    def agg_copy():
+        return pltpu.make_async_remote_copy(
+            agg_s, agg_r, as_sem.at[0], ar_sem.at[0], device_id={"ep": opposite, "tp": my_tp}
+        )
+
+    def agg_meta():
+        return pltpu.make_async_remote_copy(
+            meta_ref, meta_a, as_sem.at[1], ar_sem.at[1], device_id={"ep": opposite, "tp": my_tp}
         )
 
     def stage_a(s, rows_of):
@@ -203,18 +236,22 @@
     def stage_c(s, own):
         for o in range(1, nt):
             h_copy(s, o, True).wait_recv()
-        target = out_r if own else out_s
         for j in range(local):
             hidden = jnp.concatenate([hid[s, q, pl.ds(j * cap, cap), :] for q in range(nt)], axis=1)
-            target[s, pl.ds(j * cap, cap), :] = dot(hidden, down_v[j]).astype(BF)
+            result = dot(hidden, down_v[j]).astype(BF)
+            if own:
+                ret[0, seat, pl.ds(j * cap, cap), :] = result
+            else:
+                out_s[s, pl.ds(j * cap, cap), :] = result
         if not own:
-            o_copy(s).start()
-
-    def combine(s):
-        weight = jnp.concatenate([onehot(0, e, True) for e in experts_of(sender(s))], axis=0)
+            @pl.when(o_target(s)[1] != me)
+            def _():
+                o_copy(s).start()
+
+    def combine(slot, owner, rows):
+        weight = jnp.concatenate([onehot(slot, e, True) for e in experts_of(owner)], axis=0)
         high = weight.astype(BF)
         low = (weight - high.astype(F32)).astype(BF)
-        rows = out_r[s]
         return dot_t(high, rows) + dot_t(low, rows)
 
     values = x_ref[...].astype(F32)
@@ -224,6 +261,7 @@
     tri[...] = jnp.where(earlier, 1.0, 0.0).astype(BF)
     pl.semaphore_wait(barrier, n - 1 + nt - 1)
     send_sum(0)
+    agg_meta().start()
     if ring:
         for i in range(2):
             meta_copy(1, i).start()
@@ -313,28 +351,49 @@
 
     stage_b(n - 1)
     stage_c(n - 2, False)
-    acc[...] = combine(0)
     stage_c(n - 1, False)
+    agg_meta().wait_recv()
+    last = rank_t.shape[0] - 1
+    make_table(last, meta_a[...])
+    acc[...] = combine(last, me, out_s[opposite_step()])
+
+    @pl.loop(1, half)
+    def _(k):
+        other = lax.rem(seat + k, half)
+        o_arrival(1, other).wait_recv()
+        acc[...] += combine(last, base + other, ret[1, other])
+
+    agg_s[...] = acc[...].astype(BF)
+    acc[...] = combine(0, me, ret[0, seat])
+    agg_copy().start()
+
+    @pl.loop(1, half)
+    def _(k):
+        other = lax.rem(seat + k, half)
+        o_arrival(0, other).wait_recv()
+        acc[...] += combine(0, base + other, ret[0, other])
+
+    agg_copy().wait_recv()
+    acc[...] += agg_r[...].astype(F32)
+    summed = acc[...]
+    start_sum(1, jnp.sum(summed * summed, axis=1, keepdims=True))
+
+    @pl.loop(0, n)
+    def _(s):
+        for o in range(1, nt):
+            p_copy(s, o).wait_send()
+            h_copy(s, o).wait_send()
+
+    send_sum(1)
 
     @pl.loop(1, n)
     def _(s):
-        o_copy(s).wait_recv()
-        acc[...] += combine(s)
-
-    summed = acc[...]
-    start_sum(1, jnp.sum(summed * summed, axis=1, keepdims=True))
-
-    @pl.loop(0, n)
-    def _(s):
-        for o in range(1, nt):
-            p_copy(s, o).wait_send()
-            h_copy(s, o).wait_send()
-
-    send_sum(1)
-
-    @pl.loop(1, n)
-    def _(s):
-        o_copy(s).wait_send()
+        @pl.when(o_target(s)[1] != me)
+        def _():
+            o_copy(s).wait_send()
+
+    agg_copy().wait_send()
+    agg_meta().wait_send()
 
     if ring:
         for i in range(2):
@@ -372,7 +431,7 @@
     meta = jnp.concatenate(
         [routes.T.astype(F32), route_weights.T, jnp.zeros((4, rows), F32)], axis=0
     )
-    tables = 1 + blocks if ring else 1
+    tables = 2 + blocks if ring else 2
     packed = count + local // 2 * cap
 
     any_spec = pl.BlockSpec(memory_space=pl.ANY)
@@ -405,11 +464,14 @@
             only((2, packed, width), tiny),
             only((2, local // 2 * cap, width), tiny),
             only((blocks, 8, rows), (1, 8, 128), F32),
+            pltpu.VMEM((8, rows), F32),
             pltpu.VMEM((n, nt, count, 2 * ff // nt), BF),
             pltpu.VMEM((n, nt - 1, count, 2 * ff // nt), BF),
             pltpu.VMEM((n, nt, count, ff // nt), BF),
             pltpu.VMEM((n, count, width), BF),
-            pltpu.VMEM((n, count, width), BF),
+            pltpu.VMEM((2, n // 2, count, width), BF),
+            pltpu.VMEM((rows, width), BF),
+            pltpu.VMEM((rows, width), BF),
             dma((3,)),
             dma((blocks, 2) if ring else (n,)),
             dma((blocks, 2) if ring else (n,)),
@@ -424,9 +486,11 @@
             dma((n, nt - 1)),
             dma((n, nt - 1)),
             dma((n,)),
-            dma((n,)),
+            dma((2, n // 2)),
             dma((2, nt - 1)),
             dma((2, nt - 1)),
+            dma((2,)),
+            dma((2,)),
         ],
         compiler_params=pltpu.CompilerParams(
             collective_id=0, has_side_effects=True, vmem_limit_bytes=60 * 1024 * 1024

time: 182 us -> 200 us (1.099)
  the two profiles are of different devices: /device:TPU:11 before, /device:TPU:0 now
where the time goes in v3:
time: 200 us; the launch traced here: 199 us
  Pallas kernels  195 us (98%)
  local copies, waits for them, and re-layouts  2.34 us (1%)
  other arithmetic  2.05 us (1%)
    pallas_call x1, Pallas kernels, body(): pl.pallas_call(functools.partial(kernel, n, nt, local, cap, ring, full),...  195 us

profile of v3, /device:TPU:0, one launch (start us, length us, event | category | flops | bytes accessed | tf_op | source)
XLA Modules:
  0.0 199.4 jit_solution(10379847897400248760)
XLA Ops:
  0.0 0.1 pad.2.clone
  0.1 0.7 convert_bitcast_fusion
  0.8 1.4 maximum_maximum_fusion.meta_ref
  2.1 195.0 %shard_map.82 = bf16[512,1024]{1,0:T(8,128)(2,1)} custom-call(bf16[512,1024]{1,0:T(8,128)(2,1)} %x_ref.1, f32[8,512]{1,0:T(8,128)} %maximum_maximum_fusion.meta_ref, f32[1,1024]{1,0:T(1,128)} %bitcast.5, f32[1,1024]{1,0:T(1,128)} %bitcast.6, bf16[2,1024,512]{2,1,0:T(8,128)(2,1)} %gate_hbm.1, bf16[2,1024,512]{2,1,0:T(8,128)(2,1)} %up_hbm.1, ...), custom_call_target="tpu_custom_call" | custom-call | tf_op jit(solution)/shard_map/pallas_call | solution.py:445
  197.1 2.3 %copy.10 = bf16[512,1024]{1,0:T(8,128)(2,1)} copy(bf16[512,1024]{1,0:T(8,128)(2,1)} %shard_map.82) | data formatting | bytes 2097152
  (1 shorter events, 0.0 us)
